TPU v7x, 32 devices: a whole 2x2x4 slice. The times are simulated.
32 devices in a mesh: grp: 2 (over y), sp: 4 (over z), tp: 4 (over x, core).
Axes of the slice: x: 2, y: 2, z: 4, core: 2. Of those that a mesh axis runs over, the one named last changes fastest.
Arguments:
- query_rows: bfloat16 [4096, 1024], P(('grp', 'sp'), 'tp'), parts along dimension 0, may hold values from -128 to 128
- key_rows: bfloat16 [4096, 256], P(('grp', 'sp'), 'tp'), parts along dimension 0, may hold values from -4 to 4
- value_rows: bfloat16 [4096, 256], P(('grp', 'sp'), 'tp'), parts along dimension 0, may hold values from -6 to 6
- sink_logits: float32 [16], P('tp'), may hold values from 3 to 7
- residual: bfloat16 [4096, 2048], P(('grp', 'sp', 'tp')), parts along dimension 0, may hold values from -6 to 6
- out_weight: bfloat16 [1024, 2048], P('tp'), may hold values from -0.1875 to 0.1875
- norm_gain: float32 [2048], replicated, may hold values from 0.1 to 1.9
- gate_weight: bfloat16 [16, 2048, 512], P(('sp', 'tp')), may hold values from -0.125 to 0.125
- up_weight: bfloat16 [16, 2048, 512], P(('sp', 'tp')), may hold values from -0.125 to 0.125
- down_weight: bfloat16 [16, 512, 2048], P(('sp', 'tp')), may hold values from -0.25 to 0.25
- routes: int32 [4096, 2], P(('grp', 'sp', 'tp')), parts along dimension 0, may hold values from 0 to 15, as said below
- route_weight: float32 [4096, 2], P(('grp', 'sp', 'tp')), parts along dimension 0, may hold values from 0.1 to 1
Outputs:
- layer_out: bfloat16 [4096, 2048], P(('grp', 'sp', 'tp')), parts along dimension 0
There are 2 independent parts, one for each index of `grp`. A program takes and returns all parts, laid end to end along the dimension named above; an argument that names none is the same for every part. Nothing has to cross between parts.
Inputs may be any that keep to these rules, and one draw needn't show every extreme that they name: `routes`: A token's two experts differ and lie in the same group of 4 consecutive experts. Among the 128 tokens of one device (aligned blocks of 128 rows) no expert is named more than 32 times; in every block each expert of one group, the same group for all blocks, is named exactly 32 times.
All inputs are finite; a program needn't handle non-finite values.
Results may differ from a plain program's by a relative error of at most 0.013.
Values may be sent and summed in bfloat16 or wider, within the bound.
No kernel may reach another device: no remote copies, remote signals or barrier semaphores. Data moves between devices by JAX's collectives and lax.ppermute only.
A program may use at most 64 MiB of HBM per device.

v0:
```python
import jax
import jax.numpy as jnp
from jax import lax
from jax.sharding import PartitionSpec as P

HDIM = 64
WINDOW = 128
rope_base = 10000.0
norm_eps = 1e-06


def shifted(block, axis, distance):
    devices = range(lax.axis_size(axis))
    route = [(i - distance, i) for i in devices if i - distance in devices]
    return lax.ppermute(block, axis, route)


def rotate(rows, positions, heads):
    half_dim = HDIM // 2
    values = rows.astype(jnp.float32).reshape(rows.shape[0], heads, HDIM)
    inverse = rope_base ** (-jnp.arange(half_dim, dtype=jnp.float32) / half_dim)
    angles = positions.astype(jnp.float32)[:, None] * inverse[None, :]
    cosines = jnp.cos(angles)[:, None, :]
    sines = jnp.sin(angles)[:, None, :]
    lower = values[..., :half_dim]
    upper = values[..., half_dim:]
    turned = jnp.concatenate(
        [lower * cosines - upper * sines, upper * cosines + lower * sines], axis=-1
    )
    return turned.reshape(rows.shape[0], heads * HDIM).astype(jnp.bfloat16)


def per_device(
    query_rows,
    key_rows,
    value_rows,
    sink_logits,
    residual,
    out_weight,
    norm_gain,
    gate_weight,
    up_weight,
    down_weight,
    routes,
    route_weight,
):
    tok_count = query_rows.shape[0]
    head_local = query_rows.shape[1] // HDIM
    group_local = key_rows.shape[1] // HDIM
    repeat = head_local // group_local
    first_pos = lax.axis_index("sp") * tok_count
    positions = first_pos + jnp.arange(tok_count, dtype=jnp.int32)
    rot_q = rotate(query_rows, positions, head_local)
    rot_k = rotate(key_rows, positions, group_local)
    tails = jnp.stack([rot_k[tok_count - WINDOW :], value_rows[tok_count - WINDOW :]])
    earlier = shifted(tails, "sp", 1)
    blocks = tok_count // WINDOW
    q_blocks = rot_q.reshape(blocks, WINDOW, group_local, repeat, HDIM)
    k_blocks = rot_k.reshape(blocks, WINDOW, group_local, HDIM)
    v_blocks = value_rows.reshape(blocks, WINDOW, group_local, HDIM)
    k_prev = jnp.concatenate(
        [earlier[0].reshape(1, WINDOW, group_local, HDIM), k_blocks[:-1]], axis=0
    )
    v_prev = jnp.concatenate(
        [earlier[1].reshape(1, WINDOW, group_local, HDIM), v_blocks[:-1]], axis=0
    )
    k_wide = jnp.concatenate([k_prev, k_blocks], axis=1)
    v_wide = jnp.concatenate([v_prev, v_blocks], axis=1)
    query_pos = jnp.arange(WINDOW) + WINDOW
    key_pos = jnp.arange(2 * WINDOW)
    distance = query_pos[:, None] - key_pos[None, :]
    in_band = (distance >= 0) & (distance < WINDOW)
    key_global = (
        first_pos + jnp.arange(blocks)[:, None, None] * WINDOW + key_pos[None, None, :] - WINDOW
    )
    allowed = in_band[None] & (key_global >= 0)
    scores = jnp.einsum(
        "nqgrd,nkgd->grnqk", q_blocks, k_wide, preferred_element_type=jnp.float32
    ) * HDIM ** (-0.5)
    scores = jnp.where(allowed[None, None], scores, -jnp.inf)
    sink_here = sink_logits.reshape(group_local, repeat)[:, :, None, None, None]
    largest = jnp.maximum(scores.max(axis=-1, keepdims=True), sink_here)
    exp_scores = jnp.exp(scores - largest)
    denominator = exp_scores.sum(axis=-1, keepdims=True) + jnp.exp(sink_here - largest)
    probs = (exp_scores / denominator).astype(jnp.bfloat16)
    attended = jnp.einsum("grnqk,nkgd->nqgrd", probs, v_wide, preferred_element_type=jnp.float32)
    attended = attended.astype(jnp.bfloat16).reshape(tok_count, head_local * HDIM)
    row_count = residual.shape[0]
    token_rows = lax.all_to_all(attended, "tp", split_axis=0, concat_axis=1, tiled=True)
    projected = jnp.dot(
        token_rows,
        lax.all_gather(out_weight, "tp", axis=0, tiled=True),
        preferred_element_type=jnp.float32,
    )
    stream_f = (residual.astype(jnp.float32) + projected).astype(jnp.bfloat16).astype(jnp.float32)
    normed = (
        stream_f
        * lax.rsqrt(jnp.mean(stream_f * stream_f, axis=-1, keepdims=True) + norm_eps)
        * norm_gain[None, :]
    ).astype(jnp.bfloat16)
    sp_count = lax.axis_size("sp")
    tp_count = lax.axis_size("tp")
    expert_count = sp_count * tp_count
    capacity = 4 * row_count // expert_count
    width = normed.shape[1]
    flat_expert = routes.reshape(-1)
    one_hot = (flat_expert[:, None] == jnp.arange(expert_count, dtype=jnp.int32)[None, :]).astype(
        jnp.int32
    )
    slot_rank = jnp.sum((jnp.cumsum(one_hot, axis=0) - one_hot) * one_hot, axis=1)
    slot_index = flat_expert * capacity + slot_rank
    token_of = jnp.arange(2 * row_count, dtype=jnp.int32) // 2
    outgoing = (
        jnp.zeros((expert_count * capacity, width), jnp.bfloat16)
        .at[slot_index]
        .set(normed[token_of])
    )
    outgoing = outgoing.reshape(expert_count, capacity, width)
    arrived = lax.all_to_all(outgoing, ("sp", "tp"), split_axis=0, concat_axis=0, tiled=True)
    flat_rows = arrived.reshape(-1, width)
    gate_out = jnp.dot(flat_rows, gate_weight[0], preferred_element_type=jnp.float32)
    up_out = jnp.dot(flat_rows, up_weight[0], preferred_element_type=jnp.float32)
    hidden = (jax.nn.silu(gate_out) * up_out).astype(jnp.bfloat16)
    produced = jnp.dot(hidden, down_weight[0], preferred_element_type=jnp.float32).astype(
        jnp.bfloat16
    )
    returned = lax.all_to_all(
        produced.reshape(arrived.shape), ("sp", "tp"), split_axis=0, concat_axis=0, tiled=True
    )
    gathered = returned.reshape(expert_count * capacity, width)[slot_index].astype(jnp.float32)
    weighted = gathered * route_weight.reshape(-1)[:, None]
    combined = weighted.reshape(row_count, 2, width).sum(axis=1)
    return (stream_f + combined).astype(jnp.bfloat16)


def solution(mesh):
    in_specs = (
        P(("grp", "sp"), "tp"),
        P(("grp", "sp"), "tp"),
        P(("grp", "sp"), "tp"),
        P("tp"),
        P(("grp", "sp", "tp"), None),
        P("tp", None),
        P(),
        P(("sp", "tp"), None, None),
        P(("sp", "tp"), None, None),
        P(("sp", "tp"), None, None),
        P(("grp", "sp", "tp"), None),
        P(("grp", "sp", "tp"), None),
    )
    out_specs = P(("grp", "sp", "tp"), None)
    return jax.shard_map(
        per_device, mesh=mesh, in_specs=in_specs, out_specs=out_specs, check_vma=False
    )
```

profile of v0, /device:TPU:11, one launch (start us, length us, event | category | flops | bytes accessed | tf_op | source)
XLA Modules:
  0.0 195.3 jit_solution(5464959872850920019)
XLA Ops:
  6.5 0.7 all-gather.2.cloned.1.call-update
  7.3 0.9 bitcast_convert_fusion
  8.5 0.7 slice_bitcast_fusion.4
  9.3 3.2 %collective-permute-start = (bf16[2,128,64]{1,2,0:T(8,128)(2,1)S(1)}, bf16[2,128,64]{1,2,0:T(8,128)(2,1)S(1)}, u32[]{:S(2)}, u32[]{:S(2)}) collective-permute-start(bf16[2,128,64]{1,2,0:T(8,128)(2,1)S(1)} %pad_maximum_fusion), channel_id=1, source_target_pairs={{0,4},{4,8},{8,12},{1,5},{5,9},{9,13},{2,6},{6,10},{10,14},{3,7},{... | collective-permute-start | bytes 98312 | tf_op jit(solution)/shard_map/ppermute | solution.py:15
  12.5 0.8 copy.25
  13.8 0.6 reduce-window.6
  15.9 0.5 fusion.47
  16.9 1.2 convolution_convert_fusion.1
  18.1 4.5 %all-to-all-start = ((bf16[4,128,256]{1,2,0:T(8,128)(2,1)}), bf16[4,128,256]{1,2,0:T(8,128)(2,1)S(1)}, u32[]{:S(2)}, u32[]{:S(2)}) async-start(bf16[4,128,256]{1,2,0:T(8,128)(2,1)} %bitcast.20), calls=%async_computation | async-start | bytes 524288 | tf_op jit(solution)/shard_map/all_to_all | solution.py:89
  22.5 7.4 %all-to-all-done = bf16[4,128,256]{1,2,0:T(8,128)(2,1)S(1)} async-done(((bf16[4,128,256]{1,2,0:T(8,128)(2,1)}), bf16[4,128,256]{1,2,0:T(8,128)(2,1)S(1)}, u32[]{:S(2)}, u32[]{:S(2)}) %all-to-all-start) | async-done | bytes 262176 | tf_op jit(solution)/shard_map/all_to_all | solution.py:89
  29.9 16.9 %all-gather.2.cloned.1.call-done = bf16[1024,2048]{1,0:T(8,128)(2,1)} async-done(((bf16[256,2048]{1,0:T(8,128)(2,1)}), bf16[1024,2048]{1,0:T(8,128)(2,1)}) %all-gather.2.cloned.1.call-update) | async-done | bytes 4194320 | tf_op jit(solution)/shard_map/all_gather | solution.py:92
  46.9 3.1 %multiply_reduce_fusion.1 = (f32[128]{0:T(128)S(1)}, f32[128,2048]{1,0:T(8,128)S(1)}) fusion(bf16[128,1024]{0,1:T(8,128)(2,1)S(1)} %bitcast.116, bf16[1024,2048]{1,0:T(8,128)(2,1)} %all-gather.2.cloned.1.call-done, bf16[128,2048]{1,0:T(8,128)(2,1)} %param.16), kind=kOutput, calls=%fused_computation.25 | convolution fusion | flops 538443648 | bytes 6029824 | tf_op jit(solution)/shard_map/dot_general | solution.py:90
  50.0 1.0 multiply_convert_fusion
  51.0 7.3 %scatter_custom_fusion = bf16[512,2048]{1,0:T(8,128)(2,1)} fusion(s32[256]{0:T(256)S(1)} %bitcast.119, bf16[128,2048]{1,0:T(8,128)(2,1)} %multiply_convert_fusion, s32[1024]{0:T(1024)S(1)} %pad_clamp_fusion.1, bf16[]{:T(256)} %constant.56.clone.1), kind=kCustom, calls=%fused_computation.21 | custom fusion | bytes 2097664 | tf_op jit(solution)/shard_map/scatter | solution.py:116
  58.3 53.3 %all_to_all.29 = bf16[16,32,2048]{2,1,0:T(8,128)(2,1)S(1)} all-to-all(bf16[16,32,2048]{2,1,0:T(8,128)(2,1)} %bitcast.112), channel_id=1, replica_groups=mesh['grp'=2,'sp'=4,'tp'=4] {'sp','tp'}, dimensions={0} | all-to-all | bytes 4194304 | tf_op jit(solution)/shard_map/all_to_all | solution.py:119
  111.7 1.3 copy-done.1
  112.9 2.2 %fusion.5 = f32[512,512]{1,0:T(8,128)} fusion(bf16[512,2048]{1,0:T(8,128)(2,1)S(1)} %bitcast.114, bf16[1,2048,512]{2,1,0:T(8,128)(2,1)S(1)} %copy-done.8), kind=kOutput, calls=%fused_computation.11 | convolution fusion | flops 1073741824 | bytes 5242880 | tf_op jit(solution)/shard_map/dot_general | solution.py:121
  115.2 6.3 %convolution_convert_fusion = bf16[512,2048]{1,0:T(8,128)(2,1)} fusion(bf16[1,512,2048]{2,1,0:T(8,128)(2,1)S(1)} %copy-done, bf16[512,2048]{1,0:T(8,128)(2,1)} %bitcast.115, bf16[1,2048,512]{2,1,0:T(8,128)(2,1)} %param.20, f32[512,512]{1,0:T(8,128)} %fusion.5), kind=kOutput, calls=%fused_computation.3 | convolution fusion | flops 2150105088 | bytes 9437184 | tf_op jit(solution)/shard_map/dot_general | solution.py:124
  121.5 5.1 %all-to-all-start.2 = ((bf16[16,32,2048]{2,1,0:T(8,128)(2,1)}), bf16[16,32,2048]{2,1,0:T(8,128)(2,1)}, u32[]{:S(2)}, u32[]{:S(2)}) async-start(bf16[16,32,2048]{2,1,0:T(8,128)(2,1)} %bitcast.113), calls=%async_computation.2 | async-start | bytes 4194304 | tf_op jit(solution)/shard_map/all_to_all | solution.py:127
  126.7 47.4 %all-to-all-done.2 = bf16[16,32,2048]{2,1,0:T(8,128)(2,1)} async-done(((bf16[16,32,2048]{2,1,0:T(8,128)(2,1)}), bf16[16,32,2048]{2,1,0:T(8,128)(2,1)}, u32[]{:S(2)}, u32[]{:S(2)}) %all-to-all-start.2) | async-done | bytes 2097184 | tf_op jit(solution)/shard_map/all_to_all | solution.py:127
  174.1 5.2 %gather_fusion = bf16[256,2048]{1,0:T(8,128)(2,1)} fusion(bf16[512,2048]{1,0:T(8,128)(2,1)} %bitcast.33, s32[1024]{0:T(1024)S(1)} %pad_clamp_fusion), kind=kCustom, calls=%fused_computation.1 | custom fusion | bytes 2098176 | tf_op jit(solution)/shard_map/gather | solution.py:130
  179.3 3.4 %reshape.391 = f32[128,2,2048]{2,1,0:T(2,128)} reshape(bf16[256,2048]{1,0:T(8,128)(2,1)} %gather_fusion) | data formatting | bytes 3145728 | tf_op jit(solution)/shard_map/convert_element_type | solution.py:130
  182.7 4.8 %multiply_reduce_fusion = f32[128,2048]{1,0:T(8,128)S(1)} fusion(f32[128,2,2048]{2,1,0:T(2,128)} %reshape.391, f32[128,2]{1,0:T(8,128)S(1)} %copy.28), kind=kLoop, calls=%fused_computation.13 | loop fusion | flops 786432 | bytes 3146752 | tf_op jit(solution)/shard_map/reduce_sum | solution.py:132
  187.5 0.9 add_convert_fusion
  (62 shorter events, 2.9 us)
Async XLA Ops:
  6.5 108.6 %copy-start = (bf16[1,512,2048]{2,1,0:T(8,128)(2,1)S(1)}, bf16[1,512,2048]{2,1,0:T(8,128)(2,1)}, u32[]{:S(2)}) copy-start(bf16[1,512,2048]{2,1,0:T(8,128)(2,1)} %param.21) | copy-start | bytes 6291460
  6.5 8.2 %copy-start.5 = (s32[128,2]{0,1:T(2,128)S(1)}, s32[128,2]{0,1:T(2,128)}, u32[]{:S(2)}) copy-start(s32[128,2]{0,1:T(2,128)} %param.22) | copy-start | bytes 3076
  6.5 7.0 %copy-start.2 = (bf16[512,256]{1,0:T(8,128)(2,1)S(1)}, bf16[512,256]{1,0:T(8,128)(2,1)}, u32[]{:S(2)}) copy-start(bf16[512,256]{1,0:T(8,128)(2,1)} %param.12) | copy-start | bytes 786436
  6.5 40.3 %all-gather.2.cloned.1.call-start = ((), (), s32[]{:S(2)}) async-start(), calls=%async_computation.3 | async-start | bytes 5242880 | tf_op jit(solution)/shard_map/all_gather | solution.py:92
  7.3 8.2 %copy-start.3 = (bf16[512,64]{0,1:T(8,128)(2,1)S(1)}, bf16[512,64]{0,1:T(8,128)(2,1)}, u32[]{:S(2)}) copy-start(bf16[512,64]{0,1:T(8,128)(2,1)} %param.14) | copy-start | bytes 196612
  7.3 8.2 %slice-start = ((bf16[512,64]{0,1:T(8,128)(2,1)}), bf16[384,64]{0,1:T(8,128)(2,1)S(1)}, s32[]{:S(2)}) async-start(bf16[512,64]{0,1:T(8,128)(2,1)} %param.14), calls=%async_computation.4 | async-start | bytes 98304 | tf_op jit(solution)/shard_map/slice | solution.py:65
  9.3 6.6 %collective-permute-start = (bf16[2,128,64]{1,2,0:T(8,128)(2,1)S(1)}, bf16[2,128,64]{1,2,0:T(8,128)(2,1)S(1)}, u32[]{:S(2)}, u32[]{:S(2)}) collective-permute-start(bf16[2,128,64]{1,2,0:T(8,128)(2,1)S(1)} %pad_maximum_fusion), channel_id=1, source_target_pairs={{0,4},{4,8},{8,12},{1,5},{5,9},{9,13},{2,6},{6,10},{10,14},{3,7},{... | collective-permute-start | bytes 98312 | tf_op jit(solution)/shard_map/ppermute | solution.py:15
  15.5 0.9 copy-start.6
  18.1 11.8 %all-to-all-start = ((bf16[4,128,256]{1,2,0:T(8,128)(2,1)}), bf16[4,128,256]{1,2,0:T(8,128)(2,1)S(1)}, u32[]{:S(2)}, u32[]{:S(2)}) async-start(bf16[4,128,256]{1,2,0:T(8,128)(2,1)} %bitcast.20), calls=%async_computation | async-start | bytes 524288 | tf_op jit(solution)/shard_map/all_to_all | solution.py:89
  46.9 3.2 %copy-start.4 = (f32[2048]{0:T(1024)S(1)}, f32[2048]{0:T(1024)}, u32[]{:S(2)}) copy-start(f32[2048]{0:T(1024)} %param.18) | copy-start | bytes 24580
  58.3 54.6 %copy-start.8 = (bf16[1,2048,512]{2,1,0:T(8,128)(2,1)S(1)}, bf16[1,2048,512]{2,1,0:T(8,128)(2,1)}, u32[]{:S(2)}) copy-start(bf16[1,2048,512]{2,1,0:T(8,128)(2,1)} %param.19) | copy-start | bytes 6291460
  111.6 1.3 copy-start.1
  121.5 5.1 %copy-start.7 = (f32[128,2]{0,1:T(2,128)S(1)}, f32[128,2]{0,1:T(2,128)}, u32[]{:S(2)}) copy-start(f32[128,2]{0,1:T(2,128)} %param.23) | copy-start | bytes 3076
  121.5 52.7 %all-to-all-start.2 = ((bf16[16,32,2048]{2,1,0:T(8,128)(2,1)}), bf16[16,32,2048]{2,1,0:T(8,128)(2,1)}, u32[]{:S(2)}, u32[]{:S(2)}) async-start(bf16[16,32,2048]{2,1,0:T(8,128)(2,1)} %bitcast.113), calls=%async_computation.2 | async-start | bytes 4194304 | tf_op jit(solution)/shard_map/all_to_all | solution.py:127
Sparse Core Ops, SparseCore 0:
  8.9 37.9 all-gather.1
where the time goes:
time: 196 us; the launch traced here: 195 us
  waiting for transfers between devices  72.4 us (37%)
  blocking collectives  53.3 us (27%)
  local copies, waits for them, and re-layouts  19.8 us (10%)
  between operations  13.7 us (7%)
  matrix products  13.4 us (7%)
  starting transfers between devices  12.8 us (7%)
  other arithmetic  9.91 us (5%)
    all_to_all x1, blocking collectives, per_device(): lax.all_to_all(outgoing, ('sp', 'tp'), split_axis=0, concat_axis=0, tiled...  53.3 us
    all_to_all x1, waiting for transfers between devices, per_device(): lax.all_to_all(produced.reshape(arrived.shape), ('sp', 'tp'), split_axis=...  47.4 us
    all_gather x1, waiting for transfers between devices, per_device(): lax.all_gather(out_weight, 'tp', axis=0, tiled=True)  16.9 us
    all_to_all x1, waiting for transfers between devices, per_device(): lax.all_to_all(attended, 'tp', split_axis=0, concat_axis=1, tiled=True)  7.37 us
    scatter x1, local copies, waits for them, and re-layouts, per_device(): outgoing = jnp.zeros((expert_count * capacity, width), jnp.bfloat16).at[s...  7.33 us
    dot_general x1, matrix products, per_device(): jnp.dot(hidden, down_weight[0], preferred_element_type=jnp.float32)  6.28 us
    gather x1, local copies, waits for them, and re-layouts, per_device(): returned.reshape(expert_count * capacity, width)[slot_index]  5.2 us
    all_to_all x1, starting transfers between devices, per_device(): lax.all_to_all(produced.reshape(arrived.shape), ('sp', 'tp'), split_axis=...  5.14 us
  transfers between devices with their start and end apart: 4, of which 3 were waited for; matrix products, arithmetic and copies ran while one was open for 4% of the time, Pallas kernels for 0%

commit v1 on v0

--- a/solution.py
+++ b/solution.py
@@ -86,7 +86,10 @@
     attended = jnp.einsum("grnqk,nkgd->nqgrd", probs, v_wide, preferred_element_type=jnp.float32)
     attended = attended.astype(jnp.bfloat16).reshape(tok_count, head_local * HDIM)
     row_count = residual.shape[0]
-    token_rows = lax.all_to_all(attended, "tp", split_axis=0, concat_axis=1, tiled=True)
+    n_dev = lax.axis_size("tp")
+    pieces = jnp.stack(jnp.split(attended, n_dev, axis=0), axis=0)
+    pieces = lax.all_to_all(pieces, "tp", split_axis=0, concat_axis=0)
+    token_rows = jnp.concatenate(pieces, axis=1)
     projected = jnp.dot(
         token_rows,
         lax.all_gather(out_weight, "tp", axis=0, tiled=True),

time: 196 us -> 196 us (level)
  no operation moved by 1% of the time
where the time goes in v1:
time: 196 us; the launch traced here: 195 us
  waiting for transfers between devices  72.4 us (37%)
  blocking collectives  53.4 us (27%)
  local copies, waits for them, and re-layouts  19.8 us (10%)
  between operations  13.7 us (7%)
  starting transfers between devices  12.8 us (7%)
  matrix products  12.6 us (6%)
  other arithmetic  10.7 us (5%)
    all_to_all x1, blocking collectives, per_device(): lax.all_to_all(outgoing, ('sp', 'tp'), split_axis=0, concat_axis=0, tiled...  53.4 us
    all_to_all x1, waiting for transfers between devices, per_device(): lax.all_to_all(produced.reshape(arrived.shape), ('sp', 'tp'), split_axis=...  47.4 us
    all_gather x1, waiting for transfers between devices, per_device(): lax.all_gather(out_weight, 'tp', axis=0, tiled=True)  16.9 us
    all_to_all x1, waiting for transfers between devices, per_device(): pieces = lax.all_to_all(pieces, 'tp', split_axis=0, concat_axis=0)  7.38 us
    scatter x1, local copies, waits for them, and re-layouts, per_device(): outgoing = jnp.zeros((expert_count * capacity, width), jnp.bfloat16).at[s...  7.33 us
    dot_general x1, matrix products, per_device(): jnp.dot(hidden, down_weight[0], preferred_element_type=jnp.float32)  6.26 us
    gather x1, local copies, waits for them, and re-layouts, per_device(): returned.reshape(expert_count * capacity, width)[slot_index]  5.19 us
    all_to_all x1, starting transfers between devices, per_device(): lax.all_to_all(produced.reshape(arrived.shape), ('sp', 'tp'), split_axis=...  5.15 us
  transfers between devices with their start and end apart: 4, of which 3 were waited for; matrix products, arithmetic and copies ran while one was open for 4% of the time, Pallas kernels for 0%

profile of v1, /device:TPU:11, one launch (start us, length us, event | category | flops | bytes accessed | tf_op | source)
XLA Modules:
  0.0 195.3 jit_solution(17217919698374945270)
XLA Ops:
  6.5 0.7 all-gather.2.cloned.1.call-update
  7.3 0.9 bitcast_convert_fusion
  8.5 0.7 slice_bitcast_fusion.4
  9.3 3.2 %collective-permute-start = (bf16[2,128,64]{1,2,0:T(8,128)(2,1)S(1)}, bf16[2,128,64]{1,2,0:T(8,128)(2,1)S(1)}, u32[]{:S(2)}, u32[]{:S(2)}) collective-permute-start(bf16[2,128,64]{1,2,0:T(8,128)(2,1)S(1)} %pad_maximum_fusion.1), channel_id=1, source_target_pairs={{0,4},{4,8},{8,12},{1,5},{5,9},{9,13},{2,6},{6,10},{10,14},{3,7},{... | collective-permute-start | bytes 98312 | tf_op jit(solution)/shard_map/ppermute | solution.py:15
  12.5 0.8 copy.25
  13.8 0.6 reduce-window.6
  15.9 0.5 fusion.49
  17.4 0.7 pad_maximum_fusion
  18.1 4.5 %all-to-all-start = ((bf16[4,128,256]{1,2,0:T(8,128)(2,1)}), bf16[4,128,256]{1,2,0:T(8,128)(2,1)S(1)}, u32[]{:S(2)}, u32[]{:S(2)}) async-start(bf16[4,128,256]{1,2,0:T(8,128)(2,1)} %pad_maximum_fusion), calls=%async_computation | async-start | bytes 524288 | tf_op jit(solution)/shard_map/all_to_all | solution.py:91
  22.6 7.4 %all-to-all-done = bf16[4,128,256]{1,2,0:T(8,128)(2,1)S(1)} async-done(((bf16[4,128,256]{1,2,0:T(8,128)(2,1)}), bf16[4,128,256]{1,2,0:T(8,128)(2,1)S(1)}, u32[]{:S(2)}, u32[]{:S(2)}) %all-to-all-start) | async-done | bytes 262176 | tf_op jit(solution)/shard_map/all_to_all | solution.py:91
  30.0 16.9 %all-gather.2.cloned.1.call-done = bf16[1024,2048]{1,0:T(8,128)(2,1)} async-done(((bf16[256,2048]{1,0:T(8,128)(2,1)}), bf16[1024,2048]{1,0:T(8,128)(2,1)}) %all-gather.2.cloned.1.call-update) | async-done | bytes 4194320 | tf_op jit(solution)/shard_map/all_gather | solution.py:95
  46.9 3.1 %multiply_reduce_fusion.1 = (f32[128]{0:T(128)S(1)}, f32[128,2048]{1,0:T(8,128)S(1)}) fusion(bf16[128,1024]{0,1:T(8,128)(2,1)S(1)} %bitcast.119, bf16[1024,2048]{1,0:T(8,128)(2,1)} %all-gather.2.cloned.1.call-done, bf16[128,2048]{1,0:T(8,128)(2,1)} %param.16), kind=kOutput, calls=%fused_computation.26 | convolution fusion | flops 538443648 | bytes 6029824 | tf_op jit(solution)/shard_map/dot_general | solution.py:93
  50.0 1.0 multiply_convert_fusion
  51.0 7.3 %scatter_custom_fusion = bf16[512,2048]{1,0:T(8,128)(2,1)} fusion(s32[256]{0:T(256)S(1)} %bitcast.126, bf16[128,2048]{1,0:T(8,128)(2,1)} %multiply_convert_fusion, s32[1024]{0:T(1024)S(1)} %pad_clamp_fusion.1, bf16[]{:T(256)} %constant.56.clone.1), kind=kCustom, calls=%fused_computation.22 | custom fusion | bytes 2097664 | tf_op jit(solution)/shard_map/scatter | solution.py:119
  58.3 53.4 %all_to_all.15 = bf16[16,32,2048]{2,1,0:T(8,128)(2,1)S(1)} all-to-all(bf16[16,32,2048]{2,1,0:T(8,128)(2,1)} %bitcast.115), channel_id=1, replica_groups=mesh['grp'=2,'sp'=4,'tp'=4] {'sp','tp'}, dimensions={0} | all-to-all | bytes 4194304 | tf_op jit(solution)/shard_map/all_to_all | solution.py:122
  111.6 1.3 copy-done.1
  113.0 2.2 %fusion.5 = f32[512,512]{1,0:T(8,128)} fusion(bf16[512,2048]{1,0:T(8,128)(2,1)S(1)} %bitcast.117, bf16[1,2048,512]{2,1,0:T(8,128)(2,1)S(1)} %copy-done.8), kind=kOutput, calls=%fused_computation.11 | convolution fusion | flops 1073741824 | bytes 5242880 | tf_op jit(solution)/shard_map/dot_general | solution.py:124
  115.2 6.3 %convolution_convert_fusion = bf16[512,2048]{1,0:T(8,128)(2,1)} fusion(bf16[1,512,2048]{2,1,0:T(8,128)(2,1)S(1)} %copy-done, bf16[512,2048]{1,0:T(8,128)(2,1)} %bitcast.118, bf16[1,2048,512]{2,1,0:T(8,128)(2,1)} %param.20, f32[512,512]{1,0:T(8,128)} %fusion.5), kind=kOutput, calls=%fused_computation.3 | convolution fusion | flops 2150105088 | bytes 9437184 | tf_op jit(solution)/shard_map/dot_general | solution.py:127
  121.4 5.2 %all-to-all-start.2 = ((bf16[16,32,2048]{2,1,0:T(8,128)(2,1)}), bf16[16,32,2048]{2,1,0:T(8,128)(2,1)}, u32[]{:S(2)}, u32[]{:S(2)}) async-start(bf16[16,32,2048]{2,1,0:T(8,128)(2,1)} %bitcast.116), calls=%async_computation.2 | async-start | bytes 4194304 | tf_op jit(solution)/shard_map/all_to_all | solution.py:130
  126.7 47.4 %all-to-all-done.2 = bf16[16,32,2048]{2,1,0:T(8,128)(2,1)} async-done(((bf16[16,32,2048]{2,1,0:T(8,128)(2,1)}), bf16[16,32,2048]{2,1,0:T(8,128)(2,1)}, u32[]{:S(2)}, u32[]{:S(2)}) %all-to-all-start.2) | async-done | bytes 2097184 | tf_op jit(solution)/shard_map/all_to_all | solution.py:130
  174.1 5.2 %gather_fusion = bf16[256,2048]{1,0:T(8,128)(2,1)} fusion(bf16[512,2048]{1,0:T(8,128)(2,1)} %bitcast.37, s32[1024]{0:T(1024)S(1)} %pad_clamp_fusion), kind=kCustom, calls=%fused_computation.1 | custom fusion | bytes 2098176 | tf_op jit(solution)/shard_map/gather | solution.py:133
  179.3 3.4 %reshape.403 = f32[128,2,2048]{2,1,0:T(2,128)} reshape(bf16[256,2048]{1,0:T(8,128)(2,1)} %gather_fusion) | data formatting | bytes 3145728 | tf_op jit(solution)/shard_map/convert_element_type | solution.py:133
  182.7 4.8 %multiply_reduce_fusion = f32[128,2048]{1,0:T(8,128)S(1)} fusion(f32[128,2,2048]{2,1,0:T(2,128)} %reshape.403, f32[128,2]{1,0:T(8,128)S(1)} %copy.28), kind=kLoop, calls=%fused_computation.13 | loop fusion | flops 786432 | bytes 3146752 | tf_op jit(solution)/shard_map/reduce_sum | solution.py:135
  187.5 0.9 add_convert_fusion
  (64 shorter events, 3.4 us)
Async XLA Ops:
  6.5 108.6 %copy-start = (bf16[1,512,2048]{2,1,0:T(8,128)(2,1)S(1)}, bf16[1,512,2048]{2,1,0:T(8,128)(2,1)}, u32[]{:S(2)}) copy-start(bf16[1,512,2048]{2,1,0:T(8,128)(2,1)} %param.21) | copy-start | bytes 6291460
  6.5 8.2 %copy-start.5 = (s32[128,2]{0,1:T(2,128)S(1)}, s32[128,2]{0,1:T(2,128)}, u32[]{:S(2)}) copy-start(s32[128,2]{0,1:T(2,128)} %param.22) | copy-start | bytes 3076
  6.5 7.0 %copy-start.2 = (bf16[512,256]{1,0:T(8,128)(2,1)S(1)}, bf16[512,256]{1,0:T(8,128)(2,1)}, u32[]{:S(2)}) copy-start(bf16[512,256]{1,0:T(8,128)(2,1)} %param.12) | copy-start | bytes 786436
  6.5 40.3 %all-gather.2.cloned.1.call-start = ((), (), s32[]{:S(2)}) async-start(), calls=%async_computation.3 | async-start | bytes 5242880 | tf_op jit(solution)/shard_map/all_gather | solution.py:95
  7.3 8.2 %copy-start.3 = (bf16[512,64]{0,1:T(8,128)(2,1)S(1)}, bf16[512,64]{0,1:T(8,128)(2,1)}, u32[]{:S(2)}) copy-start(bf16[512,64]{0,1:T(8,128)(2,1)} %param.14) | copy-start | bytes 196612
  7.3 8.2 %slice-start = ((bf16[512,64]{0,1:T(8,128)(2,1)}), bf16[384,64]{0,1:T(8,128)(2,1)S(1)}, s32[]{:S(2)}) async-start(bf16[512,64]{0,1:T(8,128)(2,1)} %param.14), calls=%async_computation.4 | async-start | bytes 98304 | tf_op jit(solution)/shard_map/slice | solution.py:65
  9.3 6.6 %collective-permute-start = (bf16[2,128,64]{1,2,0:T(8,128)(2,1)S(1)}, bf16[2,128,64]{1,2,0:T(8,128)(2,1)S(1)}, u32[]{:S(2)}, u32[]{:S(2)}) collective-permute-start(bf16[2,128,64]{1,2,0:T(8,128)(2,1)S(1)} %pad_maximum_fusion.1), channel_id=1, source_target_pairs={{0,4},{4,8},{8,12},{1,5},{5,9},{9,13},{2,6},{6,10},{10,14},{3,7},{... | collective-permute-start | bytes 98312 | tf_op jit(solution)/shard_map/ppermute | solution.py:15
  15.5 0.9 copy-start.6
  18.1 11.9 %all-to-all-start = ((bf16[4,128,256]{1,2,0:T(8,128)(2,1)}), bf16[4,128,256]{1,2,0:T(8,128)(2,1)S(1)}, u32[]{:S(2)}, u32[]{:S(2)}) async-start(bf16[4,128,256]{1,2,0:T(8,128)(2,1)} %pad_maximum_fusion), calls=%async_computation | async-start | bytes 524288 | tf_op jit(solution)/shard_map/all_to_all | solution.py:91
  46.9 3.2 %copy-start.4 = (f32[2048]{0:T(1024)S(1)}, f32[2048]{0:T(1024)}, u32[]{:S(2)}) copy-start(f32[2048]{0:T(1024)} %param.18) | copy-start | bytes 24580
  58.3 54.7 %copy-start.8 = (bf16[1,2048,512]{2,1,0:T(8,128)(2,1)S(1)}, bf16[1,2048,512]{2,1,0:T(8,128)(2,1)}, u32[]{:S(2)}) copy-start(bf16[1,2048,512]{2,1,0:T(8,128)(2,1)} %param.19) | copy-start | bytes 6291460
  111.6 1.3 copy-start.1
  121.4 5.2 %copy-start.7 = (f32[128,2]{0,1:T(2,128)S(1)}, f32[128,2]{0,1:T(2,128)}, u32[]{:S(2)}) copy-start(f32[128,2]{0,1:T(2,128)} %param.23) | copy-start | bytes 3076
  121.4 52.7 %all-to-all-start.2 = ((bf16[16,32,2048]{2,1,0:T(8,128)(2,1)}), bf16[16,32,2048]{2,1,0:T(8,128)(2,1)}, u32[]{:S(2)}, u32[]{:S(2)}) async-start(bf16[16,32,2048]{2,1,0:T(8,128)(2,1)} %bitcast.116), calls=%async_computation.2 | async-start | bytes 4194304 | tf_op jit(solution)/shard_map/all_to_all | solution.py:130
Sparse Core Ops, SparseCore 0:
  8.9 37.9 all-gather.1
